TPU v7x, 32 devices: a whole 2x2x4 slice. The times are simulated.
32 devices in a mesh: sp: 4 (over y, x), tp: 8 (over z, core).
Axes of the slice: x: 2, y: 2, z: 4, core: 2. Of those that a mesh axis runs over, the one named last changes fastest.
Arguments:
- query_a: bfloat16 [512, 16, 256], P('sp', 'tp'), may hold values from -5.5 to 5.5
- key_a: bfloat16 [512, 16, 256], P('sp', 'tp'), may hold values from -5.5 to 5.5
- value_a: bfloat16 [512, 16, 256], P('sp', 'tp'), may hold values from -6 to 6
- query_b: bfloat16 [512, 16, 128], P('sp', 'tp'), may hold values from -5.5 to 5.5
- key_b: bfloat16 [512, 16, 128], P('sp', 'tp'), may hold values from -5.5 to 5.5
- value_b: bfloat16 [512, 16, 128], P('sp', 'tp'), may hold values from -6 to 6
- lambdas: float32 [2, 16], P(None, 'tp'), may hold values from 0.3 to 0.8
- gain_a: float32 [256], replicated, may hold values from 0.1 to 1.9
- gain_b: float32 [128], replicated, may hold values from 0.1 to 1.9
- out_a: bfloat16 [4096, 4096], P('tp'), may hold values from -0.078125 to 0.078125
- out_b: bfloat16 [2048, 4096], P('tp'), may hold values from -0.078125 to 0.078125
- residual: bfloat16 [512, 4096], P(('sp', 'tp')), may hold values from -6 to 6
- norm_gain: float32 [4096], replicated, may hold values from 0.1 to 1.9
- route_ids: int32 [512, 2], P(('sp', 'tp')), may hold values from 0 to 7, all different within a row; in each aligned block of 16 rows (0 to 15, 16 to 31, ...) at most 8 rows name the same one
- route_weights: float32 [512, 2], P(('sp', 'tp')), may hold values from 0.1 to 0.9
- w_gate: bfloat16 [8, 4096, 2048], P('sp', None, 'tp'), may hold values from -0.28125 to 0.28125
- w_up: bfloat16 [8, 4096, 2048], P('sp', None, 'tp'), may hold values from -0.28125 to 0.28125
- w_down: bfloat16 [8, 2048, 4096], P('sp', 'tp'), may hold values from -0.01977539 to 0.01977539
Outputs:
- result: bfloat16 [512, 4096], P(('sp', 'tp'))
Inputs may be any that keep to these rules, and one draw needn't show every extreme that they name: `route_ids`: in the rows of one device each token names 2 different experts, no expert is named more than 8 times, a bound that some block reaches.
All inputs are finite; a program needn't handle non-finite values.
Results may differ from a plain program's by a relative error of at most 0.02.
Values may be sent and summed in bfloat16 or wider, within the bound.
A program may use at most 128 MiB of HBM per device.

v0:
```python
import functools

import jax
import jax.numpy as jnp
from jax import lax
from jax.experimental import pallas as pl
from jax.experimental.pallas import tpu as pltpu
from jax.sharding import PartitionSpec as P

EPSILON = 1e-06
LIMIT = 7.0
SLOPE = 1.702
FLOOR = -1e30


def empty_state(heads_here, queries_here, value_width):
    maxima = jnp.full((2, heads_here, queries_here), FLOOR, jnp.float32)
    totals = jnp.zeros((2, heads_here, queries_here), jnp.float32)
    sums = jnp.zeros((2, heads_here, queries_here, value_width), jnp.float32)
    return (maxima, totals, sums)


def absorb_keys(states, queries, keys, values, width):
    maxima, totals, sums = states
    scaling = width ** (-0.5)
    new_maxima = []
    new_totals = []
    new_sums = []
    for which in range(2):
        query_part = queries[:, :, which * width : (which + 1) * width]
        key_part = keys[:, :, which * width : (which + 1) * width]
        scores = (
            jnp.einsum("qhd,khd->hqk", query_part, key_part, preferred_element_type=jnp.float32)
            * scaling
        )
        highest = jnp.maximum(maxima[which], jnp.max(scores, axis=2))
        expo = jnp.exp(scores - highest[:, :, None])
        factor = jnp.exp(maxima[which] - highest)
        new_totals.append(totals[which] * factor + jnp.sum(expo, axis=2))
        carried = jnp.einsum(
            "hqk,khv->hqv", expo.astype(jnp.bfloat16), values, preferred_element_type=jnp.float32
        )
        new_sums.append(sums[which] * factor[:, :, None] + carried)
        new_maxima.append(highest)
    return (jnp.stack(new_maxima), jnp.stack(new_totals), jnp.stack(new_sums))


def finish(states, lambda_row, gain):
    maxima, totals, sums = states
    heard = sums / totals[:, :, :, None]
    differ = heard[0] - lambda_row[:, None, None] * heard[1]
    scaled = lax.rsqrt(jnp.mean(differ * differ, axis=2, keepdims=True) + EPSILON)
    return (differ * scaled * gain).astype(jnp.bfloat16)


def gated_units(grid, w_gate, w_up):
    gate = jnp.einsum("necd,edf->necf", grid, w_gate, preferred_element_type=jnp.float32)
    upward = jnp.einsum("necd,edf->necf", grid, w_up, preferred_element_type=jnp.float32)
    clamped = jnp.minimum(gate, LIMIT)
    return (
        clamped * jax.nn.sigmoid(SLOPE * clamped) * (jnp.clip(upward, -LIMIT, LIMIT) + 1.0)
    ).astype(jnp.bfloat16)


def per_device_plain(
    query_a,
    key_a,
    value_a,
    query_b,
    key_b,
    value_b,
    lambdas,
    gain_a,
    gain_b,
    out_a,
    out_b,
    residual,
    norm_gain,
    route_ids,
    route_weights,
    w_gate,
    w_up,
    w_down,
):
    heads_here = query_a.shape[1]
    queries_here = query_a.shape[0]
    width_a = query_a.shape[2] // 2
    width_b = query_b.shape[2] // 2
    starting = (
        empty_state(heads_here, queries_here, value_a.shape[2]),
        empty_state(heads_here, queries_here, value_b.shape[2]),
    )
    keys_a = lax.all_gather(key_a, "sp", axis=0, tiled=True)
    values_a = lax.all_gather(value_a, "sp", axis=0, tiled=True)
    keys_b = lax.all_gather(key_b, "sp", axis=0, tiled=True)
    values_b = lax.all_gather(value_b, "sp", axis=0, tiled=True)
    state_a = absorb_keys(starting[0], query_a, keys_a, values_a, width_a)
    state_b = absorb_keys(starting[1], query_b, keys_b, values_b, width_b)
    attended_a = finish(state_a, lambdas[0], gain_a)
    attended_b = finish(state_b, lambdas[1], gain_b)
    model_width = out_a.shape[1]
    weights_a = out_a.reshape(heads_here, -1, model_width)
    weights_b = out_b.reshape(heads_here, -1, model_width)
    first = jnp.einsum("hqv,hvd->qd", attended_a, weights_a, preferred_element_type=jnp.float32)
    projected = lax.psum_scatter(
        (
            first
            + jnp.einsum("hqv,hvd->qd", attended_b, weights_b, preferred_element_type=jnp.float32)
        ).astype(jnp.bfloat16),
        "tp",
        scatter_dimension=0,
        tiled=True,
    ).astype(jnp.float32)
    mixed = (residual.astype(jnp.float32) + projected).astype(jnp.bfloat16)
    widened = mixed.astype(jnp.float32)
    normed = (
        widened
        * lax.rsqrt(jnp.mean(widened * widened, axis=1, keepdims=True) + EPSILON)
        * norm_gain
    ).astype(jnp.bfloat16)
    rows_here, chosen = route_ids.shape
    groups = lax.axis_size("sp")
    experts_here = w_gate.shape[0]
    experts_all = experts_here * groups
    capacity = 2 * rows_here * chosen // experts_all
    slots_here = experts_here * capacity
    flat_ids = route_ids.reshape(-1)
    onehot = (flat_ids[:, None] == jnp.arange(experts_all, dtype=jnp.int32)[None, :]).astype(
        jnp.int32
    )
    earlier = jnp.cumsum(onehot, axis=0) - onehot
    target = flat_ids * capacity + jnp.sum(earlier * onehot, axis=1)
    places = jnp.arange(experts_all * capacity, dtype=jnp.int32)
    layout = jnp.any(target.reshape(rows_here, chosen)[None, :, :] == places[:, None, None], axis=2)
    outgoing = jnp.dot(
        layout.astype(jnp.bfloat16), normed, preferred_element_type=jnp.float32
    ).astype(jnp.bfloat16)
    outgoing = outgoing.reshape(groups, slots_here, model_width)
    arrived = lax.all_to_all(outgoing, "sp", split_axis=0, concat_axis=0, tiled=True)
    pieces = lax.all_gather(arrived, "tp", axis=0, tiled=True)
    count = pieces.shape[0]
    grid = pieces.reshape(count, experts_here, capacity, model_width)
    active = gated_units(grid, w_gate, w_up)
    down = jnp.einsum("necf,efd->necd", active, w_down, preferred_element_type=jnp.float32)
    partial_value = down.astype(jnp.bfloat16).reshape(count, slots_here, model_width)
    totals = lax.psum_scatter(
        partial_value.astype(jnp.float32).astype(jnp.bfloat16),
        "tp",
        scatter_dimension=0,
        tiled=True,
    )
    summed = lax.all_to_all(totals, "sp", split_axis=0, concat_axis=0, tiled=True)
    results = summed.reshape(experts_all * capacity, model_width)
    picked = (
        jnp.take(results, target, axis=0)
        .reshape(rows_here, chosen, model_width)
        .astype(jnp.float32)
    )
    combined = jnp.sum(route_weights[:, :, None] * picked, axis=1)
    return (widened + combined).astype(jnp.bfloat16)


def layer_kernel(
    dims,
    kv_ref,
    q_ref,
    lam_ref,
    gain_a_ref,
    gain_b_ref,
    res_ref,
    norm_ref,
    route_ref,
    out_a_hbm,
    out_b_hbm,
    gate_hbm,
    up_hbm,
    down_hbm,
    o_ref,
    kv_all,
    out_a,
    out_b,
    w_gate,
    w_up,
    w_down,
    att_a,
    att_b,
    part,
    pair1,
    sum1,
    z1,
    mixed,
    x_all,
    act,
    contrib,
    pair2,
    red,
    sp2,
    z2s,
    z2,
    tot,
    loc_sem,
    kv_s,
    kv_r,
    p1_s,
    p1_r,
    z1_s,
    z1_r,
    gz_s,
    gz_r,
    gs_s,
    gs_r,
    gp_s,
    gp_r,
    p2_s,
    p2_r,
    s2_s,
    s2_r,
    z2_s,
    z2_r,
):
    n_sp, n_tp, heads, da, db, va, vb = dims
    nz = n_tp // 2
    f32, bf16 = jnp.float32, jnp.bfloat16
    sp = lax.axis_index("sp")
    tp = lax.axis_index("tp")
    z, core = tp // 2, tp % 2
    rows, width = res_ref.shape
    chunk = n_sp * 2 * rows
    experts_here, _, hidden = w_gate.shape
    experts_all = experts_here * n_sp

    def sp_at(e):
        return lax.rem(sp + e + n_sp, n_sp)

    def z_at(d):
        return lax.rem(z + d + nz, nz)

    partner = {"sp": sp, "tp": z * 2 + 1 - core}

    def to_sp(e):
        return {"sp": sp_at(e), "tp": tp}

    def to_z(d):
        return {"sp": sp, "tp": z_at(d) * 2 + core}

    def remote(src, dst, send, recv, device):
        return pltpu.make_async_remote_copy(
            src_ref=src,
            dst_ref=dst,
            send_sem=send,
            recv_sem=recv,
            device_id=device,
            device_id_type=pl.DeviceIdType.MESH,
        )

    x_next = sp + 1 - 2 * (sp % 2)
    y_next = lax.rem(sp + 2, n_sp)

    def kv_copy(i):
        owner, target, half = (
            (sp, x_next, 0),
            (sp, y_next, 1),
            (sp, x_next, 1),
            (sp, y_next, 0),
            (x_next, y_next, 0),
            (y_next, x_next, 1),
        )[i]
        size = kv_ref.shape[0] // 2
        part_rows = pl.ds(half * size, size)
        place = kv_all.at[owner, part_rows]
        source = kv_ref.at[part_rows] if i < 4 else place
        return remote(source, place, kv_s.at[i], kv_r.at[i], {"sp": target, "tp": tp})

    def p1_copy(d):
        zz = z_at(d)
        return remote(part.at[1 - core, zz], pair1.at[zz], p1_s.at[d], p1_r.at[d], partner)

    def z1_copy(d):
        return remote(sum1.at[z_at(d)], z1.at[d - 1], z1_s.at[d - 1], z1_r.at[d - 1], to_z(d))

    def gz_copy(d):
        block = x_all.at[z, sp, core]
        return remote(block, block, gz_s.at[d - 1], gz_r.at[d - 1], to_z(d))

    def gs_copy(e, d):
        block = x_all.at[z_at(-d), sp, core]
        return remote(block, block, gs_s.at[e - 1, d], gs_r.at[e - 1, d], to_sp(e))

    def gp_copy(e, d):
        block = x_all.at[z_at(-d), sp_at(-e), core]
        return remote(block, block, gp_s.at[e, d], gp_r.at[e, d], partner)

    def p2_copy(d):
        return remote(contrib.at[d, 1 - core], pair2.at[d], p2_s.at[d], p2_r.at[d], partner)

    def s2_copy(e, d):
        return remote(
            red.at[d, sp_at(e)], sp2.at[e - 1, d], s2_s.at[e - 1, d], s2_r.at[e - 1, d], to_sp(e)
        )

    def z2_copy(d):
        return remote(z2s.at[d - 1], z2.at[d - 1], z2_s.at[d - 1], z2_r.at[d - 1], to_z(-d))

    barrier = pltpu.get_barrier_semaphore()
    for e in range(1, n_sp):
        pl.semaphore_signal(
            barrier, inc=1, device_id=to_sp(e), device_id_type=pl.DeviceIdType.MESH
        )
    for d in range(1, nz):
        pl.semaphore_signal(barrier, inc=1, device_id=to_z(d), device_id_type=pl.DeviceIdType.MESH)
    pl.semaphore_signal(barrier, inc=1, device_id=partner, device_id_type=pl.DeviceIdType.MESH)
    pl.semaphore_wait(barrier, n_sp - 1 + nz - 1 + 1)

    for i in range(4):
        kv_copy(i).start()
    loads = [
        pltpu.make_async_copy(src, dst, loc_sem.at[i])
        for i, (src, dst) in enumerate(
            (
                (kv_ref, kv_all.at[sp]),
                (out_a_hbm, out_a),
                (out_b_hbm, out_b),
                (gate_hbm, w_gate),
                (up_hbm, w_up),
                (down_hbm, w_down),
            )
        )
    ]
    for load in loads:
        load.start()
    loads[0].wait()
    for i in range(2):
        kv_copy(i).wait_recv()
        kv_copy(4 + i).start()
    for i in range(2, 6):
        kv_copy(i).wait_recv()

    positions = kv_all.shape[1] * n_sp

    def attend(q0, k0, v0, map_width, value_width, lam, gain):
        heard = []
        for which in range(2):
            if map_width % 128 == 0:
                query = q_ref[:, q0 + which * map_width : q0 + (which + 1) * map_width]
                keys = kv_all[:, :, k0 + which * map_width : k0 + (which + 1) * map_width]
            else:
                query = q_ref[:, q0 : q0 + 2 * map_width]
                lane = lax.broadcasted_iota(jnp.int32, query.shape, 1)
                inside = (lane >= which * map_width) & (lane < (which + 1) * map_width)
                query = jnp.where(inside, query.astype(f32), 0.0).astype(bf16)
                keys = kv_all[:, :, k0 : k0 + 2 * map_width]
            keys = keys.reshape(positions, keys.shape[2])
            scores = lax.dot_general(
                query, keys, (((1,), (1,)), ((), ())), preferred_element_type=f32
            ) * (map_width**-0.5)
            expo = jnp.exp(scores - jnp.max(scores, axis=1, keepdims=True))
            total = jnp.sum(expo, axis=1, keepdims=True)
            values = kv_all[:, :, v0 : v0 + value_width].reshape(positions, value_width)
            carried = jnp.dot(expo.astype(bf16), values, preferred_element_type=f32)
            heard.append(carried / total)
        differ = heard[0] - lam * heard[1]
        scaled = lax.rsqrt(jnp.mean(differ * differ, axis=1, keepdims=True) + EPSILON)
        return (differ * scaled * gain).astype(bf16)

    base_va = heads * 2 * da
    base_kb = base_va + heads * va
    base_vb = base_kb + heads * 2 * db
    for h in range(heads):
        att_a[:, h * va : (h + 1) * va] = attend(
            h * 2 * da, h * 2 * da, base_va + h * va, da, va, lam_ref[0, h], gain_a_ref[...]
        )
    for h in range(heads):
        att_b[:, h * vb : (h + 1) * vb] = attend(
            heads * 2 * da + h * 2 * db,
            base_kb + h * 2 * db,
            base_vb + h * vb,
            db,
            vb,
            lam_ref[1, h],
            gain_b_ref[...],
        )

    loads[1].wait()
    loads[2].wait()
    tile = 512

    @pl.loop(0, width // tile)
    def _(j):
        cols = pl.ds(pl.multiple_of(j * tile, tile), tile)
        value = jnp.dot(att_a[...], out_a[:, cols], preferred_element_type=f32) + jnp.dot(
            att_b[...], out_b[:, cols], preferred_element_type=f32
        )
        value = value.astype(bf16)
        for zz in range(nz):
            for c in range(2):
                r = (zz * 2 + c) * rows
                part[c, zz, :, cols] = value[r : r + rows]

    order = list(range(1, nz)) + [0]
    for d in order:
        p1_copy(d).start()
    for d in order:
        p1_copy(d).wait_recv()
        zz = z_at(d)
        both = part[core, zz].astype(f32) + pair1[zz].astype(f32)
        if d > 0:
            sum1[zz] = both.astype(bf16)
            z1_copy(d).start()
        else:
            tot[...] = both
    for d in range(1, nz):
        z1_copy(d).wait_recv()
        tot[...] += z1[d - 1].astype(f32)
    mix = (res_ref[...].astype(f32) + tot[...]).astype(bf16)
    mixed[...] = mix
    wide = mix.astype(f32)
    scaled = lax.rsqrt(jnp.mean(wide * wide, axis=1, keepdims=True) + EPSILON)
    x_all[z, sp, core, :, :width] = (wide * scaled * norm_ref[...]).astype(bf16)
    route = route_ref[...]
    high = route.astype(bf16)
    lane = lax.broadcasted_iota(jnp.int32, route.shape, 1)
    x_all[z, sp, core, :, width:] = jnp.where(
        lane < experts_all, high.astype(f32), route - high.astype(f32)
    ).astype(bf16)

    for d in range(1, nz):
        gz_copy(d).start()
    for e in range(1, n_sp):
        gs_copy(e, 0).start()
    gp_copy(0, 0).start()
    for load in loads[3:]:
        load.wait()

    def settle(d):
        total = red[d, sp].astype(f32)
        for e in range(1, n_sp):
            s2_copy(e, d).wait_recv()
            total += sp2[e - 1, d].astype(f32)

        @pl.when(d > 0)
        def _():
            z2s[d - 1] = total.astype(bf16)
            z2_copy(d).start()

        @pl.when(d == 0)
        def _():
            tot[...] = total

    @pl.loop(0, nz)
    def _(d):
        @pl.when(d + 1 < nz)
        def _():
            gz_copy(d + 1).wait_recv()
            for e in range(1, n_sp):
                gs_copy(e, d + 1).start()
            gp_copy(0, d + 1).start()

        for e in range(1, n_sp):
            gs_copy(e, d).wait_recv()
            gp_copy(e, d).start()
        for e in range(n_sp):
            gp_copy(e, d).wait_recv()
        zz = z_at(-d)
        share = x_all[zz, :, :, :, width:].reshape(chunk, route.shape[1]).astype(f32)
        lanes = lax.broadcasted_iota(jnp.int32, share.shape, 1)
        for j in range(experts_here):
            which = sp * experts_here + j
            weight = jnp.sum(
                jnp.where((lanes == which) | (lanes == which + experts_all), share, 0.0),
                axis=1,
                keepdims=True,
            )
            x = x_all[zz, :, :, :, :width].reshape(chunk, width)
            gate = jnp.dot(x, w_gate[j], preferred_element_type=f32)
            upward = jnp.dot(x, w_up[j], preferred_element_type=f32)
            clamped = jnp.minimum(gate, LIMIT)
            active = (
                clamped * jax.nn.sigmoid(SLOPE * clamped) * (jnp.clip(upward, -LIMIT, LIMIT) + 1.0)
            )
            act[:, j * hidden : (j + 1) * hidden] = (active * weight).astype(bf16)

        @pl.loop(0, width // tile)
        def _(i):
            cols = pl.ds(pl.multiple_of(i * tile, tile), tile)
            rowsum = jnp.zeros((chunk, tile), f32)
            for j in range(experts_here):
                rowsum += jnp.dot(
                    act[:, j * hidden : (j + 1) * hidden],
                    w_down[j, :, cols],
                    preferred_element_type=f32,
                )
            value = rowsum.astype(bf16)
            for s in range(n_sp):
                for c in range(2):
                    r = (s * 2 + c) * rows
                    contrib[d, c, s, :, cols] = value[r : r + rows]

        p2_copy(d).start()
        p2_copy(d).wait_recv()
        for e in list(range(1, n_sp)) + [0]:
            s = sp_at(e)
            red[d, s] = (contrib[d, core, s].astype(f32) + pair2[d, s].astype(f32)).astype(bf16)
            if e > 0:
                s2_copy(e, d).start()

        @pl.when(d > 0)
        def _():
            settle(d - 1)

    settle(nz - 1)
    for d in range(1, nz):
        z2_copy(d).wait_recv()
        tot[...] += z2[d - 1].astype(f32)
    o_ref[...] = (mixed[...].astype(f32) + tot[...]).astype(bf16)

    for i in range(6):
        kv_copy(i).wait_send()
    for d in range(nz):
        p1_copy(d).wait_send()
    for d in range(1, nz):
        z1_copy(d).wait_send()
        gz_copy(d).wait_send()
        z2_copy(d).wait_send()
    for d in range(nz):
        p2_copy(d).wait_send()
        for e in range(n_sp):
            gp_copy(e, d).wait_send()
            if e > 0:
                gs_copy(e, d).wait_send()
                s2_copy(e, d).wait_send()


def per_device(
    n_sp,
    n_tp,
    query_a,
    key_a,
    value_a,
    query_b,
    key_b,
    value_b,
    lambdas,
    gain_a,
    gain_b,
    out_a,
    out_b,
    residual,
    norm_gain,
    route_ids,
    route_weights,
    w_gate,
    w_up,
    w_down,
):
    here, heads, _ = query_a.shape
    da, db = query_a.shape[2] // 2, query_b.shape[2] // 2
    va, vb = value_a.shape[2], value_b.shape[2]
    rows, width = residual.shape
    experts_here, _, hidden = w_gate.shape
    experts_all = experts_here * n_sp
    nz = n_tp // 2
    bf16, f32 = jnp.bfloat16, jnp.float32

    def flat(*arrays):
        return jnp.concatenate([a.reshape(here, -1) for a in arrays], axis=1)

    kv = flat(key_a, value_a, key_b, value_b)
    queries = flat(query_a, query_b)
    chosen = route_ids[:, :, None] == jnp.arange(experts_all, dtype=jnp.int32)
    dense = jnp.sum(jnp.where(chosen, route_weights[:, :, None], 0.0), axis=1)
    lanes = -(-2 * experts_all // 128) * 128
    route = jnp.concatenate(
        [dense, dense, jnp.zeros((rows, lanes - 2 * experts_all), f32)], axis=1
    )
    vmem = pl.BlockSpec(memory_space=pltpu.VMEM)
    hbm = pl.BlockSpec(memory_space=pl.ANY)
    sem = pltpu.SemaphoreType.DMA
    pairs = [(6,), (nz,), (nz - 1,), (nz - 1,), (n_sp - 1, nz), (n_sp, nz), (nz,)]
    pairs += [(n_sp - 1, nz), (nz - 1,)]
    scratch = [
        pltpu.VMEM((n_sp,) + kv.shape, bf16),
        pltpu.VMEM(out_a.shape, bf16),
        pltpu.VMEM(out_b.shape, bf16),
        pltpu.VMEM(w_gate.shape, bf16),
        pltpu.VMEM(w_up.shape, bf16),
        pltpu.VMEM(w_down.shape, bf16),
        pltpu.VMEM((here, heads * va), bf16),
        pltpu.VMEM((here, heads * vb), bf16),
        pltpu.VMEM((2, nz, rows, width), bf16),
        pltpu.VMEM((nz, rows, width), bf16),
        pltpu.VMEM((nz, rows, width), bf16),
        pltpu.VMEM((nz - 1, rows, width), bf16),
        pltpu.VMEM((rows, width), bf16),
        pltpu.VMEM((nz, n_sp, 2, rows, width + lanes), bf16),
        pltpu.VMEM((n_sp * 2 * rows, experts_here * hidden), bf16),
        pltpu.VMEM((nz, 2, n_sp, rows, width), bf16),
        pltpu.VMEM((nz, n_sp, rows, width), bf16),
        pltpu.VMEM((nz, n_sp, rows, width), bf16),
        pltpu.VMEM((n_sp - 1, nz, rows, width), bf16),
        pltpu.VMEM((nz - 1, rows, width), bf16),
        pltpu.VMEM((nz - 1, rows, width), bf16),
        pltpu.VMEM((rows, width), f32),
        sem((6,)),
    ]
    for shape in pairs:
        scratch += [sem(shape), sem(shape)]
    return pl.pallas_call(
        functools.partial(layer_kernel, (n_sp, n_tp, heads, da, db, va, vb)),
        out_shape=jax.ShapeDtypeStruct((rows, width), bf16),
        in_specs=[vmem, vmem, pl.BlockSpec(memory_space=pltpu.SMEM)] + [vmem] * 5 + [hbm] * 5,
        out_specs=vmem,
        scratch_shapes=scratch,
        compiler_params=pltpu.CompilerParams(
            collective_id=0, has_side_effects=True, vmem_limit_bytes=60 * 1024 * 1024
        ),
    )(
        kv,
        queries,
        lambdas,
        gain_a.reshape(1, -1),
        gain_b.reshape(1, -1),
        residual,
        norm_gain.reshape(1, -1),
        route,
        out_a,
        out_b,
        w_gate,
        w_up,
        w_down,
    )


def solution(mesh):
    in_specs = (
        P("sp", "tp", None),
        P("sp", "tp", None),
        P("sp", "tp", None),
        P("sp", "tp", None),
        P("sp", "tp", None),
        P("sp", "tp", None),
        P(None, "tp"),
        P(),
        P(),
        P("tp", None),
        P("tp", None),
        P(("sp", "tp"), None),
        P(),
        P(("sp", "tp"), None),
        P(("sp", "tp"), None),
        P("sp", None, "tp"),
        P("sp", None, "tp"),
        P("sp", "tp", None),
    )
    out_specs = P(("sp", "tp"), None)
    n_sp, n_tp = mesh.shape["sp"], mesh.shape["tp"]
    fits = n_sp == 4 and n_tp % 2 == 0 and n_tp <= 8
    body = functools.partial(per_device, n_sp, n_tp) if fits else per_device_plain
    return jax.shard_map(
        body, mesh=mesh, in_specs=in_specs, out_specs=out_specs, check_vma=False
    )
```

profile of v0, /device:TPU:0, one launch (start us, length us, event | category | flops | bytes accessed | tf_op | source)
XLA Modules:
  0.0 108.5 jit_solution(17779126632419140675)
XLA Ops:
  0.0 0.9 copy_bitcast_fusion.1
  0.9 0.9 copy.23
  1.8 0.9 copy.24
  2.7 0.8 pad_maximum_fusion.kv_ref
  3.5 0.9 copy.27
  4.4 0.9 copy.32
  5.3 0.7 pad_maximum_fusion.1.q_ref
  6.0 0.7 select_reduce_fusion
  6.7 0.1 copy.21
  6.7 0.1 pad.2.clone
  6.8 0.7 maximum_maximum_fusion.route_ref
  7.5 99.5 %shard_map.172 = bf16[16,4096]{1,0:T(8,128)(2,1)} custom-call(bf16[128,1536]{1,0:T(8,128)(2,1)} %pad_maximum_fusion.kv_ref, bf16[128,768]{1,0:T(8,128)(2,1)} %pad_maximum_fusion.1.q_ref, f32[2,2]{1,0:T(2,128)} %lam_ref.1, f32[1,256]{1,0:T(1,128)} %bitcast.30, f32[1,128]{1,0:T(1,128)} %bitcast.31, bf16[16,4096]{1,0:T(8,128)(2,1)} %res_ref.1, ...), custom_call_target="tpu_custom_call" | custom-call | tf_op jit(solution)/shard_map/pallas_call | solution.py:607
  107.0 1.6 %copy.34 = bf16[16,4096]{1,0:T(8,128)(2,1)} copy(bf16[16,4096]{1,0:T(8,128)(2,1)} %shard_map.172) | data formatting | bytes 262144
  (1 shorter events, 0.0 us)
where the time goes:
time: 109 us
  Pallas kernels  99.5 us (91%)
  local copies, waits for them, and re-layouts  6.22 us (6%)
  other arithmetic  2.83 us (3%)
    pallas_call x1, Pallas kernels, per_device(): pl.pallas_call(functools.partial(layer_kernel, (n_sp, n_tp, heads, da, db...  99.5 us
    unnamed x5, local copies, waits for them, and re-layouts  5.18 us

commit v1 on v0

v1 whole, which is shorter than its diff:
```python
import functools

import jax
import jax.numpy as jnp
from jax import lax
from jax.experimental import pallas as pl
from jax.experimental.pallas import tpu as pltpu
from jax.sharding import PartitionSpec as P

EPSILON = 1e-06
LIMIT = 7.0
SLOPE = 1.702
FLOOR = -1e30


def empty_state(heads_here, queries_here, value_width):
    maxima = jnp.full((2, heads_here, queries_here), FLOOR, jnp.float32)
    totals = jnp.zeros((2, heads_here, queries_here), jnp.float32)
    sums = jnp.zeros((2, heads_here, queries_here, value_width), jnp.float32)
    return (maxima, totals, sums)


def absorb_keys(states, queries, keys, values, width):
    maxima, totals, sums = states
    scaling = width ** (-0.5)
    new_maxima = []
    new_totals = []
    new_sums = []
    for which in range(2):
        query_part = queries[:, :, which * width : (which + 1) * width]
        key_part = keys[:, :, which * width : (which + 1) * width]
        scores = (
            jnp.einsum("qhd,khd->hqk", query_part, key_part, preferred_element_type=jnp.float32)
            * scaling
        )
        highest = jnp.maximum(maxima[which], jnp.max(scores, axis=2))
        expo = jnp.exp(scores - highest[:, :, None])
        factor = jnp.exp(maxima[which] - highest)
        new_totals.append(totals[which] * factor + jnp.sum(expo, axis=2))
        carried = jnp.einsum(
            "hqk,khv->hqv", expo.astype(jnp.bfloat16), values, preferred_element_type=jnp.float32
        )
        new_sums.append(sums[which] * factor[:, :, None] + carried)
        new_maxima.append(highest)
    return (jnp.stack(new_maxima), jnp.stack(new_totals), jnp.stack(new_sums))


def finish(states, lambda_row, gain):
    maxima, totals, sums = states
    heard = sums / totals[:, :, :, None]
    differ = heard[0] - lambda_row[:, None, None] * heard[1]
    scaled = lax.rsqrt(jnp.mean(differ * differ, axis=2, keepdims=True) + EPSILON)
    return (differ * scaled * gain).astype(jnp.bfloat16)


def gated_units(grid, w_gate, w_up):
    gate = jnp.einsum("necd,edf->necf", grid, w_gate, preferred_element_type=jnp.float32)
    upward = jnp.einsum("necd,edf->necf", grid, w_up, preferred_element_type=jnp.float32)
    clamped = jnp.minimum(gate, LIMIT)
    return (
        clamped * jax.nn.sigmoid(SLOPE * clamped) * (jnp.clip(upward, -LIMIT, LIMIT) + 1.0)
    ).astype(jnp.bfloat16)


def per_device_plain(
    query_a,
    key_a,
    value_a,
    query_b,
    key_b,
    value_b,
    lambdas,
    gain_a,
    gain_b,
    out_a,
    out_b,
    residual,
    norm_gain,
    route_ids,
    route_weights,
    w_gate,
    w_up,
    w_down,
):
    heads_here = query_a.shape[1]
    queries_here = query_a.shape[0]
    width_a = query_a.shape[2] // 2
    width_b = query_b.shape[2] // 2
    starting = (
        empty_state(heads_here, queries_here, value_a.shape[2]),
        empty_state(heads_here, queries_here, value_b.shape[2]),
    )
    keys_a = lax.all_gather(key_a, "sp", axis=0, tiled=True)
    values_a = lax.all_gather(value_a, "sp", axis=0, tiled=True)
    keys_b = lax.all_gather(key_b, "sp", axis=0, tiled=True)
    values_b = lax.all_gather(value_b, "sp", axis=0, tiled=True)
    state_a = absorb_keys(starting[0], query_a, keys_a, values_a, width_a)
    state_b = absorb_keys(starting[1], query_b, keys_b, values_b, width_b)
    attended_a = finish(state_a, lambdas[0], gain_a)
    attended_b = finish(state_b, lambdas[1], gain_b)
    model_width = out_a.shape[1]
    weights_a = out_a.reshape(heads_here, -1, model_width)
    weights_b = out_b.reshape(heads_here, -1, model_width)
    first = jnp.einsum("hqv,hvd->qd", attended_a, weights_a, preferred_element_type=jnp.float32)
    projected = lax.psum_scatter(
        (
            first
            + jnp.einsum("hqv,hvd->qd", attended_b, weights_b, preferred_element_type=jnp.float32)
        ).astype(jnp.bfloat16),
        "tp",
        scatter_dimension=0,
        tiled=True,
    ).astype(jnp.float32)
    mixed = (residual.astype(jnp.float32) + projected).astype(jnp.bfloat16)
    widened = mixed.astype(jnp.float32)
    normed = (
        widened
        * lax.rsqrt(jnp.mean(widened * widened, axis=1, keepdims=True) + EPSILON)
        * norm_gain
    ).astype(jnp.bfloat16)
    rows_here, chosen = route_ids.shape
    groups = lax.axis_size("sp")
    experts_here = w_gate.shape[0]
    experts_all = experts_here * groups
    capacity = 2 * rows_here * chosen // experts_all
    slots_here = experts_here * capacity
    flat_ids = route_ids.reshape(-1)
    onehot = (flat_ids[:, None] == jnp.arange(experts_all, dtype=jnp.int32)[None, :]).astype(
        jnp.int32
    )
    earlier = jnp.cumsum(onehot, axis=0) - onehot
    target = flat_ids * capacity + jnp.sum(earlier * onehot, axis=1)
    places = jnp.arange(experts_all * capacity, dtype=jnp.int32)
    layout = jnp.any(target.reshape(rows_here, chosen)[None, :, :] == places[:, None, None], axis=2)
    outgoing = jnp.dot(
        layout.astype(jnp.bfloat16), normed, preferred_element_type=jnp.float32
    ).astype(jnp.bfloat16)
    outgoing = outgoing.reshape(groups, slots_here, model_width)
    arrived = lax.all_to_all(outgoing, "sp", split_axis=0, concat_axis=0, tiled=True)
    pieces = lax.all_gather(arrived, "tp", axis=0, tiled=True)
    count = pieces.shape[0]
    grid = pieces.reshape(count, experts_here, capacity, model_width)
    active = gated_units(grid, w_gate, w_up)
    down = jnp.einsum("necf,efd->necd", active, w_down, preferred_element_type=jnp.float32)
    partial_value = down.astype(jnp.bfloat16).reshape(count, slots_here, model_width)
    totals = lax.psum_scatter(
        partial_value.astype(jnp.float32).astype(jnp.bfloat16),
        "tp",
        scatter_dimension=0,
        tiled=True,
    )
    summed = lax.all_to_all(totals, "sp", split_axis=0, concat_axis=0, tiled=True)
    results = summed.reshape(experts_all * capacity, model_width)
    picked = (
        jnp.take(results, target, axis=0)
        .reshape(rows_here, chosen, model_width)
        .astype(jnp.float32)
    )
    combined = jnp.sum(route_weights[:, :, None] * picked, axis=1)
    return (widened + combined).astype(jnp.bfloat16)


def layer_kernel(
    dims,
    lam_ref,
    ids_ref,
    wts_ref,
    qa_hbm,
    ka_hbm,
    va_hbm,
    qb_hbm,
    kb_hbm,
    vb_hbm,
    gain_a_hbm,
    gain_b_hbm,
    res_hbm,
    norm_hbm,
    out_a_hbm,
    out_b_hbm,
    gate_hbm,
    up_hbm,
    down_hbm,
    o_ref,
    qa_raw,
    ka_raw,
    va_raw,
    qb_raw,
    kb_raw,
    vb_raw,
    gain_a,
    gain_b,
    res,
    norm,
    out_a,
    out_b,
    w_gate,
    w_up,
    w_down,
    spread,
    query_a,
    query_b,
    kv_all,
    att_a,
    att_b,
    acc,
    route,
    part,
    pair1,
    sum1,
    z1,
    tot,
    mixed,
    x_all,
    act,
    contrib,
    pair2,
    red,
    r1,
    mid,
    r2,
    home,
    z2s,
    z2,
    loc_sem,
    kv_s,
    kv_r,
    p1_s,
    p1_r,
    z1_s,
    z1_r,
    gz_s,
    gz_r,
    gs_s,
    gs_r,
    gp_s,
    gp_r,
    p2_s,
    p2_r,
    r1_s,
    r1_r,
    r2_s,
    r2_r,
    z2_s,
    z2_r,
):
    n_sp, n_tp, heads, da, db, va, vb = dims
    nz = n_tp // 2
    f32, bf16 = jnp.float32, jnp.bfloat16
    sp = lax.axis_index("sp")
    tp = lax.axis_index("tp")
    z, core = tp // 2, tp % 2
    rows, width = res.shape
    halves = part.shape[0]
    band = rows // halves
    steps = halves * nz
    chunk = 2 * n_sp * 2 * band
    lanes = route.shape[1]
    wide = width + lanes
    cut = -(-wide // 256) * 128
    side = width // 2
    here = query_a.shape[0]
    experts_here, _, hidden = w_gate.shape
    experts_all = experts_here * n_sp

    x_next = sp + 1 - 2 * (sp % 2)
    y_next = lax.rem(sp + 2, n_sp)
    corner = n_sp - 1 - sp

    def z_at(d):
        return lax.rem(z + d + nz, nz)

    partner = {"sp": sp, "tp": z * 2 + 1 - core}
    to_x = {"sp": x_next, "tp": tp}
    to_y = {"sp": y_next, "tp": tp}

    def to_z(d):
        return {"sp": sp, "tp": z_at(d) * 2 + core}

    def remote(src, dst, send, recv, device):
        return pltpu.make_async_remote_copy(
            src_ref=src,
            dst_ref=dst,
            send_sem=send,
            recv_sem=recv,
            device_id=device,
            device_id_type=pl.DeviceIdType.MESH,
        )

    distant = halves * (nz - 1)

    def step_of(h, d):
        return h * (nz - 1) + d - 1 if d > 0 else distant + h

    def kv_copy(p, i):
        owner, target, half = (
            (sp, to_x, 0),
            (sp, to_y, 1),
            (sp, to_x, 1),
            (sp, to_y, 0),
            (x_next, to_y, 0),
            (y_next, to_x, 1),
        )[i]
        size = here // 2
        place = kv_all.at[p, owner, pl.ds(half * size, size)]
        return remote(place, place, kv_s.at[p, i], kv_r.at[p, i], target)

    def p1_copy(h):
        return remote(part.at[h, 1 - core], pair1.at[h], p1_s.at[h], p1_r.at[h], partner)

    def z1_copy(h, d):
        return remote(
            sum1.at[h, z_at(d)], z1.at[h, d - 1], z1_s.at[h, d - 1], z1_r.at[h, d - 1], to_z(d)
        )

    def gz_copy(h, d):
        return remote(
            x_all.at[step_of(h, 0), sp, core],
            x_all.at[step_of(h, d), sp, core],
            gz_s.at[step_of(h, d)],
            gz_r.at[step_of(h, d)],
            to_z(d),
        )

    def gs_copy(k, i):
        owner, target, half = (
            (sp, to_x, 0),
            (sp, to_y, 1),
            (sp, to_x, 1),
            (sp, to_y, 0),
            (x_next, to_y, 0),
            (y_next, to_x, 1),
        )[i]
        cols = pl.ds(0, cut) if half == 0 else pl.ds(cut, wide - cut)
        place = x_all.at[k, owner, core, :, cols]
        return remote(place, place, gs_s.at[k, i], gs_r.at[k, i], target)

    def gp_copy(k, e):
        block = x_all.at[k, (sp, x_next, y_next, corner)[e], core]
        return remote(block, block, gp_s.at[k, e], gp_r.at[k, e], partner)

    def p2_copy(k):
        return remote(contrib.at[k, 1 - core], pair2.at[k], p2_s.at[k], p2_r.at[k], partner)

    def r1_copy(k, i):
        owner, target, first = (
            (corner, to_x, True),
            (corner, to_y, False),
            (x_next, to_x, True),
            (y_next, to_y, False),
        )[i]
        cols = pl.ds(0, side) if first else pl.ds(side, side)
        return remote(
            red.at[k, owner, :, cols], r1.at[k, i], r1_s.at[k, i], r1_r.at[k, i], target
        )

    def r2_copy(k, i):
        return remote(mid.at[k, i], r2.at[k, i], r2_s.at[k, i], r2_r.at[k, i], (to_y, to_x)[i])

    def z2_copy(k):
        return remote(z2s.at[k], z2.at[k], z2_s.at[k], z2_r.at[k], to_z(-(k % (nz - 1) + 1)))

    moves = (
        (kb_hbm, kb_raw),
        (vb_hbm, vb_raw),
        (ka_hbm, ka_raw),
        (va_hbm, va_raw),
        (qb_hbm, qb_raw),
        (qa_hbm, qa_raw),
        (gain_a_hbm, gain_a),
        (gain_b_hbm, gain_b),
        (out_b_hbm, out_b),
        (out_a_hbm, out_a),
        (res_hbm, res),
        (norm_hbm, norm),
        (gate_hbm, w_gate),
        (up_hbm, w_up),
        (down_hbm, w_down),
    )
    loads = [
        pltpu.make_async_copy(src, dst, loc_sem.at[i]) for i, (src, dst) in enumerate(moves)
    ]
    barrier = pltpu.get_barrier_semaphore()
    greeted = [to_x, to_y, partner] + [to_z(d) for d in range(1, nz)]
    for device in greeted:
        pl.semaphore_signal(
            barrier, inc=1, device_id=device, device_id_type=pl.DeviceIdType.MESH
        )
    for load in loads:
        load.start()

    def deal(raw, out, base, slots):
        count = raw.shape[0]
        spread[:count] = raw[...].astype(f32)
        stride = count // here
        for i in range(stride):
            column = base + slots(i)
            out[:, column : column + 128] = spread[pl.ds(i, here, stride=stride), :].astype(bf16)

    loads[0].wait()
    loads[1].wait()
    own_b = kv_all.at[0, sp]
    deal(kb_raw, own_b, 0, lambda i: i * 128)
    deal(vb_raw, own_b, heads * 2 * db, lambda i: i * 128)
    pl.semaphore_wait(barrier, len(greeted))
    for i in range(4):
        kv_copy(0, i).start()

    def deal_a(raw, base):
        count = raw.shape[0]
        spread[:count] = raw[...].astype(f32)
        stride = count // here
        for i in range(stride):
            c, h = i // heads, i % heads
            column = base + c * 128
            kv_all[1 + h, sp, :, column : column + 128] = spread[
                pl.ds(i, here, stride=stride), :
            ].astype(bf16)

    loads[2].wait()
    deal_a(ka_raw, 0)
    loads[3].wait()
    deal_a(va_raw, 2 * da)
    for i in range(4):
        kv_copy(1, i).start()
    loads[4].wait()
    deal(qb_raw, query_b, 0, lambda i: i * 128)
    loads[5].wait()
    deal(qa_raw, query_a, 0, lambda i: (i % heads) * 2 * da + (i // heads) * 128)
    lane = lax.broadcasted_iota(jnp.int32, (1, lanes), 1)
    folded = jnp.where(lane < experts_all, lane, lane - experts_all)
    for r in range(rows):
        row = jnp.zeros((1, lanes), f32)
        for j in range(ids_ref.shape[0]):
            row += jnp.where(folded == ids_ref[j, r], wts_ref[j, r], 0.0)
        route[r : r + 1, :] = row

    for i in range(2):
        kv_copy(0, i).wait_recv()
        kv_copy(0, 4 + i).start()
    for p in range(2, 1 + heads):
        for i in range(4):
            kv_copy(p, i).start()
    for i in range(2):
        kv_copy(1, i).wait_recv()
        kv_copy(1, 4 + i).start()

    positions = here * n_sp

    def attend(p, q_ref, q0, k0, v0, map_width, value_width, lam, gain):
        heard = []
        for which in range(2):
            if map_width % 128 == 0:
                query = q_ref[:, q0 + which * map_width : q0 + (which + 1) * map_width]
                keys = kv_all[p, :, :, k0 + which * map_width : k0 + (which + 1) * map_width]
            else:
                query = q_ref[:, q0 : q0 + 2 * map_width]
                at = lax.broadcasted_iota(jnp.int32, query.shape, 1)
                inside = (at >= which * map_width) & (at < (which + 1) * map_width)
                query = jnp.where(inside, query.astype(f32), 0.0).astype(bf16)
                keys = kv_all[p, :, :, k0 : k0 + 2 * map_width]
            keys = keys.reshape(positions, keys.shape[2])
            scores = lax.dot_general(
                query, keys, (((1,), (1,)), ((), ())), preferred_element_type=f32
            ) * (map_width**-0.5)
            expo = jnp.exp(scores - jnp.max(scores, axis=1, keepdims=True))
            total = jnp.sum(expo, axis=1, keepdims=True)
            values = kv_all[p, :, :, v0 : v0 + value_width].reshape(positions, value_width)
            carried = jnp.dot(expo.astype(bf16), values, preferred_element_type=f32)
            heard.append(carried / total)
        differ = heard[0] - lam * heard[1]
        scaled = lax.rsqrt(jnp.mean(differ * differ, axis=1, keepdims=True) + EPSILON)
        return (differ * scaled * gain).astype(bf16)

    def attend_a(h):
        att_a[:, h * va : (h + 1) * va] = attend(
            1 + h, query_a, h * 2 * da, 0, 2 * da, da, va, lam_ref[0, h], gain_a[...]
        )

    for load in loads[6:10]:
        load.wait()
    for i in range(2, 6):
        kv_copy(0, i).wait_recv()
    for h in range(heads):
        att_b[:, h * vb : (h + 1) * vb] = attend(
            0,
            query_b,
            h * 2 * db,
            h * 2 * db,
            heads * 2 * db + h * vb,
            db,
            vb,
            lam_ref[1, h],
            gain_b[...],
        )
    for p in range(2, 1 + heads):
        for i in range(2):
            kv_copy(p, i).wait_recv()
            kv_copy(p, 4 + i).start()
    for h in range(heads - 1):
        for i in range(2, 6):
            kv_copy(1 + h, i).wait_recv()
        attend_a(h)
    tile, group = 512, 4
    known = (heads - 1) * va

    @pl.loop(0, width // (tile * group))
    def _(i):
        for g in range(group):
            cols = pl.ds(pl.multiple_of((i * group + g) * tile, tile), tile)
            acc[:, cols] = jnp.dot(
                att_a[:, :known], out_a[:known, cols], preferred_element_type=f32
            ) + jnp.dot(att_b[...], out_b[:, cols], preferred_element_type=f32)

    for i in range(2, 6):
        kv_copy(heads, i).wait_recv()
    attend_a(heads - 1)

    @pl.loop(0, width // (tile * group))
    def _(i):
        for g in range(group):
            cols = pl.ds(pl.multiple_of((i * group + g) * tile, tile), tile)
            value = acc[:, cols] + jnp.dot(
                att_a[:, known:], out_a[known:, cols], preferred_element_type=f32
            )
            value = value.astype(bf16)
            for zz in range(nz):
                for c in range(2):
                    for h in range(halves):
                        r = (zz * 2 + c) * rows + h * band
                        part[h, c, zz, :, cols] = value[r : r + band]

    for h in range(halves):
        p1_copy(h).start()
    loads[10].wait()
    loads[11].wait()

    def fold(h):
        p1_copy(h).wait_recv()
        for d in range(1, nz):
            zz = z_at(d)
            sum1[h, zz] = (part[h, core, zz].astype(f32) + pair1[h, zz].astype(f32)).astype(bf16)
            if h == 0:
                z1_copy(h, d).start()
        tot[h] = part[h, core, z].astype(f32) + pair1[h, z].astype(f32)

    fold(0)
    fold(1)

    def normalise(h):
        total = tot[h]
        for d in range(1, nz):
            z1_copy(h, d).wait_recv()
            total += z1[h, d - 1].astype(f32)
        here_rows = slice(h * band, (h + 1) * band)
        mix = (res[here_rows].astype(f32) + total).astype(bf16)
        mixed[h] = mix
        full = mix.astype(f32)
        scaled = lax.rsqrt(jnp.mean(full * full, axis=1, keepdims=True) + EPSILON)
        x_all[step_of(h, 0), sp, core, :, :width] = (full * scaled * norm[...]).astype(bf16)
        weights = route[here_rows]
        high = weights.astype(bf16).astype(f32)
        at = lax.broadcasted_iota(jnp.int32, weights.shape, 1)
        x_all[step_of(h, 0), sp, core, :, width:] = jnp.where(
            at < experts_all, high, weights - high
        ).astype(bf16)
        for d in range(1, nz):
            gz_copy(h, d).start()

    def arrive(k):
        block = x_all.at[k, sp, core]
        remote(block, block, gz_s.at[k], gz_r.at[k], to_z(1)).wait_recv()

    def open_step(k):
        for i in range(4):
            gs_copy(k, i).start()
        gp_copy(k, 0).start()

    def relay(k):
        for i in range(2):
            gs_copy(k, i).wait_recv()
            gs_copy(k, 4 + i).start()

    def collect(k):
        gs_copy(k, 2).wait_recv()
        gp_copy(k, 1).start()
        gs_copy(k, 3).wait_recv()
        gp_copy(k, 2).start()
        gs_copy(k, 4).wait_recv()
        gs_copy(k, 5).wait_recv()
        gp_copy(k, 3).start()

    def compute(q):
        for i in range(2):
            for e in range(4):
                gp_copy(2 * q + i, e).wait_recv()
        both = pl.ds(2 * q, 2)
        share = x_all[both, :, :, :, width:].reshape(chunk, lanes).astype(f32)
        at = lax.broadcasted_iota(jnp.int32, share.shape, 1)
        x = x_all[both, :, :, :, :width].reshape(chunk, width)
        for j in range(experts_here):
            which = sp * experts_here + j
            weight = jnp.sum(
                jnp.where((at == which) | (at == which + experts_all), share, 0.0),
                axis=1,
                keepdims=True,
            )
            gate = jnp.dot(x, w_gate[j], preferred_element_type=f32)
            upward = jnp.dot(x, w_up[j], preferred_element_type=f32)
            clamped = jnp.minimum(gate, LIMIT)
            active = (
                clamped * jax.nn.sigmoid(SLOPE * clamped) * (jnp.clip(upward, -LIMIT, LIMIT) + 1.0)
            )
            act[:, j * hidden : (j + 1) * hidden] = (active * weight).astype(bf16)

        @pl.loop(0, width // (tile * group))
        def _(i):
            for g in range(group):
                cols = pl.ds(pl.multiple_of((i * group + g) * tile, tile), tile)
                rowsum = jnp.zeros((chunk, tile), f32)
                for j in range(experts_here):
                    rowsum += jnp.dot(
                        act[:, j * hidden : (j + 1) * hidden],
                        w_down[j, :, cols],
                        preferred_element_type=f32,
                    )
                value = rowsum.astype(bf16)
                for t in range(2):
                    for s in range(n_sp):
                        for c in range(2):
                            r = ((t * n_sp + s) * 2 + c) * band
                            contrib[2 * q + t, c, s, :, cols] = value[r : r + band]

        for i in range(2):
            p2_copy(2 * q + i).start()

    first_cols, last_cols = slice(0, side), slice(side, 2 * side)

    def join(k, s, cols):
        red[k, s, :, cols] = (
            contrib[k, core, s, :, cols].astype(f32) + pair2[k, s, :, cols].astype(f32)
        ).astype(bf16)

    def reduce_out(k):
        p2_copy(k).wait_recv()
        join(k, corner, first_cols)
        r1_copy(k, 0).start()
        join(k, corner, last_cols)
        r1_copy(k, 1).start()
        join(k, x_next, first_cols)
        r1_copy(k, 2).start()
        join(k, y_next, last_cols)
        r1_copy(k, 3).start()

    def reduce_mid(k):
        join(k, y_next, first_cols)
        join(k, x_next, last_cols)
        r1_copy(k, 0).wait_recv()
        mid[k, 0] = (red[k, y_next, :, first_cols].astype(f32) + r1[k, 0].astype(f32)).astype(bf16)
        r2_copy(k, 0).start()
        r1_copy(k, 1).wait_recv()
        mid[k, 1] = (red[k, x_next, :, last_cols].astype(f32) + r1[k, 1].astype(f32)).astype(bf16)
        r2_copy(k, 1).start()

    def reduce_in(k):
        for i, cols in enumerate((first_cols, last_cols)):
            total = contrib[k, core, sp, :, cols].astype(f32) + pair2[k, sp, :, cols].astype(f32)
            r1_copy(k, 2 + i).wait_recv()
            r2_copy(k, i).wait_recv()
            total += r1[k, 2 + i].astype(f32) + r2[k, i].astype(f32)

            @pl.when(k < distant)
            def _():
                z2s[k, :, cols] = total.astype(bf16)

            @pl.when(k >= distant)
            def _():
                home[k - distant, :, cols] = total

        @pl.when(k < distant)
        def _():
            z2_copy(k).start()

    normalise(0)
    open_step(distant)
    for d in range(1, nz):
        z1_copy(1, d).start()
    arrive(0)
    open_step(0)
    relay(distant)
    arrive(1)
    open_step(1)
    relay(0)
    for load in loads[12:]:
        load.wait()

    @pl.loop(0, steps + 4)
    def _(k):
        @pl.when(k + 2 < distant)
        def _():
            arrive(k + 2)
            open_step(k + 2)

        @pl.when(k + 1 < distant)
        def _():
            relay(k + 1)

        @pl.when(k == 2)
        def _():
            relay(distant + 1)

        @pl.when(k < steps)
        def _():
            collect(k)

        @pl.when((k >= 2) & (k - 2 < steps))
        def _():
            reduce_out(k - 2)

        @pl.when((k >= 3) & (k - 3 < steps))
        def _():
            reduce_mid(k - 3)

        @pl.when(k >= 4)
        def _():
            reduce_in(k - 4)

        @pl.when(k == 0)
        def _():
            normalise(1)
            open_step(distant + 1)

        @pl.when((k < steps) & (k % 2 == 1))
        def _():
            compute(k // 2)

    for h in range(halves):
        total = mixed[h].astype(f32) + home[h]
        for d in range(1, nz):
            k = step_of(h, d)
            z2_copy(k).wait_recv()
            total += z2[k].astype(f32)
        o_ref[h * band : (h + 1) * band, :] = total.astype(bf16)

    for p in range(1 + heads):
        for i in range(6):
            kv_copy(p, i).wait_send()
    for h in range(halves):
        p1_copy(h).wait_send()
        for d in range(1, nz):
            z1_copy(h, d).wait_send()
            gz_copy(h, d).wait_send()
            z2_copy(step_of(h, d)).wait_send()

    @pl.loop(0, steps)
    def _(k):
        for i in range(6):
            gs_copy(k, i).wait_send()
        for e in range(4):
            gp_copy(k, e).wait_send()
            r1_copy(k, e).wait_send()
        p2_copy(k).wait_send()
        for i in range(2):
            r2_copy(k, i).wait_send()


def per_device(
    n_sp,
    n_tp,
    query_a,
    key_a,
    value_a,
    query_b,
    key_b,
    value_b,
    lambdas,
    gain_a,
    gain_b,
    out_a,
    out_b,
    residual,
    norm_gain,
    route_ids,
    route_weights,
    w_gate,
    w_up,
    w_down,
):
    here, heads, _ = query_a.shape
    da, db = query_a.shape[2] // 2, query_b.shape[2] // 2
    va, vb = value_a.shape[2], value_b.shape[2]
    rows, width = residual.shape
    experts_here, _, hidden = w_gate.shape
    experts_all = experts_here * n_sp
    nz = n_tp // 2
    bf16, f32 = jnp.bfloat16, jnp.float32

    def raw(array):
        pieces = array.shape[2] // 128
        split = array.reshape(here, heads, pieces, 128)
        return split.transpose(0, 2, 1, 3).reshape(here * pieces * heads, 128)

    streams = [raw(a) for a in (query_a, key_a, value_a, query_b, key_b, value_b)]
    lanes = -(-2 * experts_all // 128) * 128
    halves = 2
    band = rows // halves
    steps = halves * nz
    kv_width = 2 * da + va
    assert heads * (2 * db + vb) == kv_width and 2 * db == 128 and vb == 128
    hbm = pl.BlockSpec(memory_space=pl.ANY)
    smem = pl.BlockSpec(memory_space=pltpu.SMEM)
    sem = pltpu.SemaphoreType.DMA
    pairs = [(1 + heads, 6), (halves,), (halves, nz - 1), (halves * (nz - 1),), (steps, 6)]
    pairs += [(steps, 4), (steps,), (steps, 4), (steps, 2), (halves * (nz - 1),)]
    scratch = [pltpu.VMEM(a.shape, bf16) for a in streams]
    scratch += [
        pltpu.VMEM((1, va), f32),
        pltpu.VMEM((1, vb), f32),
        pltpu.VMEM((rows, width), bf16),
        pltpu.VMEM((1, width), f32),
        pltpu.VMEM(out_a.shape, bf16),
        pltpu.VMEM(out_b.shape, bf16),
        pltpu.VMEM(w_gate.shape, bf16),
        pltpu.VMEM(w_up.shape, bf16),
        pltpu.VMEM(w_down.shape, bf16),
        pltpu.VMEM((max(a.shape[0] for a in streams), 128), f32),
        pltpu.VMEM((here, heads * 2 * da), bf16),
        pltpu.VMEM((here, heads * 2 * db), bf16),
        pltpu.VMEM((1 + heads, n_sp, here, kv_width), bf16),
        pltpu.VMEM((here, heads * va), bf16),
        pltpu.VMEM((here, heads * vb), bf16),
        pltpu.VMEM((here, width), f32),
        pltpu.VMEM((rows, lanes), f32),
        pltpu.VMEM((halves, 2, nz, band, width), bf16),
        pltpu.VMEM((halves, nz, band, width), bf16),
        pltpu.VMEM((halves, nz, band, width), bf16),
        pltpu.VMEM((halves, nz - 1, band, width), bf16),
        pltpu.VMEM((halves, band, width), f32),
        pltpu.VMEM((halves, band, width), bf16),
        pltpu.VMEM((steps, n_sp, 2, band, width + lanes), bf16),
        pltpu.VMEM((2 * n_sp * 2 * band, experts_here * hidden), bf16),
        pltpu.VMEM((steps, 2, n_sp, band, width), bf16),
        pltpu.VMEM((steps, n_sp, band, width), bf16),
        pltpu.VMEM((steps, n_sp, band, width), bf16),
        pltpu.VMEM((steps, 4, band, width // 2), bf16),
        pltpu.VMEM((steps, 2, band, width // 2), bf16),
        pltpu.VMEM((steps, 2, band, width // 2), bf16),
        pltpu.VMEM((halves, band, width), f32),
        pltpu.VMEM((halves * (nz - 1), band, width), bf16),
        pltpu.VMEM((halves * (nz - 1), band, width), bf16),
        sem((15,)),
    ]
    for shape in pairs:
        scratch += [sem(shape), sem(shape)]
    return pl.pallas_call(
        functools.partial(layer_kernel, (n_sp, n_tp, heads, da, db, va, vb)),
        out_shape=jax.ShapeDtypeStruct((rows, width), bf16),
        in_specs=[smem] * 3 + [hbm] * 15,
        out_specs=pl.BlockSpec(memory_space=pltpu.VMEM),
        scratch_shapes=scratch,
        compiler_params=pltpu.CompilerParams(
            collective_id=0, has_side_effects=True, vmem_limit_bytes=60 * 1024 * 1024
        ),
    )(
        lambdas,
        route_ids.T,
        route_weights.T,
        *streams,
        gain_a.reshape(1, -1),
        gain_b.reshape(1, -1),
        residual,
        norm_gain.reshape(1, -1),
        out_a,
        out_b,
        w_gate,
        w_up,
        w_down,
    )


def solution(mesh):
    in_specs = (
        P("sp", "tp", None),
        P("sp", "tp", None),
        P("sp", "tp", None),
        P("sp", "tp", None),
        P("sp", "tp", None),
        P("sp", "tp", None),
        P(None, "tp"),
        P(),
        P(),
        P("tp", None),
        P("tp", None),
        P(("sp", "tp"), None),
        P(),
        P(("sp", "tp"), None),
        P(("sp", "tp"), None),
        P("sp", None, "tp"),
        P("sp", None, "tp"),
        P("sp", "tp", None),
    )
    out_specs = P(("sp", "tp"), None)
    n_sp, n_tp = mesh.shape["sp"], mesh.shape["tp"]
    fits = n_sp == 4 and n_tp % 2 == 0 and n_tp <= 8
    body = functools.partial(per_device, n_sp, n_tp) if fits else per_device_plain
    return jax.shard_map(
        body, mesh=mesh, in_specs=in_specs, out_specs=out_specs, check_vma=False
    )
```

time: 109 us -> 90.9 us (0.83)
  Pallas kernels: 99.5 us -> 89.1 us
  local copies, waits for them, and re-layouts: 6.22 us -> 1.57 us
  other arithmetic: 2.83 us -> 0 us
    pallas_call x1, Pallas kernels: 99.5 us -> 89.1 us  [per_device(): pl.pallas_call(functools.partial(layer_kernel, (n_sp, n_tp, heads, da, db...]
    unnamed x5 -> x1, local copies, waits for them, and re-layouts: 5.18 us -> 1.57 us
    concatenate x3 -> x0, other arithmetic: 2.12 us -> none  [the longest x2 1.45 us: flat(): return jnp.concatenate([a.reshape(here, -1) for a in arrays], axis=1)]
where the time goes in v1:
time: 90.9 us; the launch traced here: 90.7 us
  Pallas kernels  89.1 us (98%)
  local copies, waits for them, and re-layouts  1.57 us (2%)
    pallas_call x1, Pallas kernels, per_device(): pl.pallas_call(functools.partial(layer_kernel, (n_sp, n_tp, heads, da, db...  89.1 us

profile of v1, /device:TPU:0, one launch (start us, length us, event | category | flops | bytes accessed | tf_op | source)
XLA Modules:
  0.0 90.7 jit_solution(16991963873860208549)
XLA Ops:
  0.0 89.1 %shard_map.172 = bf16[16,4096]{1,0:T(8,128)(2,1)} custom-call(f32[2,2]{1,0:T(2,128)} %lam_ref.1, s32[2,16]{1,0:T(2,128)} %bitcast.30, f32[2,16]{1,0:T(2,128)} %bitcast.31, bf16[512,128]{1,0:T(8,128)(2,1)} %bitcast.23, bf16[512,128]{1,0:T(8,128)(2,1)} %bitcast.24, bf16[512,128]{1,0:T(8,128)(2,1)} %bitcast.25, bf16[256,128]{1,0:T(8,128)(2,1)} %bitcast.26, ...), custom_call_target="tpu_custom_call" | custom-call | tf_op jit(solution)/shard_map/pallas_call | solution.py:854
  89.1 1.6 %copy.23 = bf16[16,4096]{1,0:T(8,128)(2,1)} copy(bf16[16,4096]{1,0:T(8,128)(2,1)} %shard_map.172) | data formatting | bytes 262144

commit v2 on v1

--- a/solution.py
+++ b/solution.py
@@ -160,6 +160,15 @@
     return (widened + combined).astype(jnp.bfloat16)
 
 
+PLAN = (
+    ("n0 o0 z a1", "o1 f0 f1 a2", "o2 n1 o7 c1", "a3 o3 c0 f2", "f7 a4 o4 c2", "f3 a5 o5 w",),
+    ("f4 c3 f5 c7", "a6 o6 r1",),
+    ("c5 f6 c4 r2", "r3 m1",),
+    ("c6 m2 m3 r5", "r4",),
+    ("i2 m5 i1 r6", "m4 i3 i5 m6", "r0 r7 i4 i6", "m0 m7 i0 i7",),
+)
+
+
 def layer_kernel(
     dims,
     lam_ref,
@@ -239,7 +248,6 @@
     r1_s,
     r1_r,
     r2_s,
-    r2_r,
     z2_s,
     z2_r,
 ):
@@ -253,12 +261,12 @@
     halves = part.shape[0]
     band = rows // halves
     steps = halves * nz
-    chunk = 2 * n_sp * 2 * band
     lanes = route.shape[1]
     wide = width + lanes
     cut = -(-wide // 256) * 128
     side = width // 2
     here = query_a.shape[0]
+    chunk = 2 * n_sp * 2 * band
     experts_here, _, hidden = w_gate.shape
     experts_all = experts_here * n_sp
 
@@ -286,10 +294,24 @@
             device_id_type=pl.DeviceIdType.MESH,
         )
 
-    distant = halves * (nz - 1)
-
-    def step_of(h, d):
-        return h * (nz - 1) + d - 1 if d > 0 else distant + h
+    def rank(at, owner):
+        low = owner - jnp.where(owner > at, 1, 0)
+        high = nz - 1 - owner - jnp.where(owner < at, 1, 0)
+        return jnp.where(2 * at < nz, low, high)
+
+    def owner_of(r):
+        low = r + jnp.where(r >= z, 1, 0)
+        high = nz - 1 - r - jnp.where(r >= nz - 1 - z, 1, 0)
+        return jnp.where(2 * z < nz, low, high)
+
+    def own_step(h):
+        return 0 if h == 0 else h * nz + nz - 1
+
+    def far_steps(h):
+        return range(1, nz) if h == 0 else range(h * nz, h * nz + nz - 1)
+
+    def settle(ref, sem):
+        pltpu.make_async_copy(ref, ref, sem).wait()
 
     def kv_copy(p, i):
         owner, target, half = (
@@ -302,24 +324,40 @@
         )[i]
         size = here // 2
         place = kv_all.at[p, owner, pl.ds(half * size, size)]
-        return remote(place, place, kv_s.at[p, i], kv_r.at[p, i], target)
+        return remote(place, place, kv_s, kv_r.at[p, min(i, 2)], target)
 
     def p1_copy(h):
-        return remote(part.at[h, 1 - core], pair1.at[h], p1_s.at[h], p1_r.at[h], partner)
+        return remote(part.at[h, 1 - core], pair1.at[h], p1_s, p1_r.at[h], partner)
 
     def z1_copy(h, d):
         return remote(
-            sum1.at[h, z_at(d)], z1.at[h, d - 1], z1_s.at[h, d - 1], z1_r.at[h, d - 1], to_z(d)
-        )
-
-    def gz_copy(h, d):
+            sum1.at[h, z_at(d)], z1.at[h, d - 1], z1_s, z1_r.at[h], to_z(d)
+        )
+
+    def gz_copy(k, owner, target, send):
+        there = far_steps(k // nz)[0] + rank(target, owner)
         return remote(
-            x_all.at[step_of(h, 0), sp, core],
-            x_all.at[step_of(h, d), sp, core],
-            gz_s.at[step_of(h, d)],
-            gz_r.at[step_of(h, d)],
-            to_z(d),
-        )
+            x_all.at[k, sp, core],
+            x_all.at[there, sp, core],
+            gz_s.at[send],
+            gz_r.at[there],
+            {"sp": sp, "tp": target * 2 + core},
+        )
+
+    def spread_z(h, act):
+        for i, target in enumerate((z + 1, z - 1)):
+
+            @pl.when((target >= 0) & (target < nz))
+            def _():
+                act(gz_copy(own_step(h), z, target, halves * nz + 2 * h + i))
+
+    def pass_on(k, act):
+        owner = owner_of(k - far_steps(k // nz)[0])
+        target = jnp.where(owner < z, z + 1, z - 1)
+
+        @pl.when((target >= 0) & (target < nz))
+        def _():
+            act(gz_copy(k, owner, target, k))
 
     def gs_copy(k, i):
         owner, target, half = (
@@ -332,14 +370,21 @@
         )[i]
         cols = pl.ds(0, cut) if half == 0 else pl.ds(cut, wide - cut)
         place = x_all.at[k, owner, core, :, cols]
-        return remote(place, place, gs_s.at[k, i], gs_r.at[k, i], target)
+        return remote(place, place, gs_s, gs_r.at[k, min(i, 2)], target)
 
     def gp_copy(k, e):
         block = x_all.at[k, (sp, x_next, y_next, corner)[e], core]
-        return remote(block, block, gp_s.at[k, e], gp_r.at[k, e], partner)
-
-    def p2_copy(k):
-        return remote(contrib.at[k, 1 - core], pair2.at[k], p2_s.at[k], p2_r.at[k], partner)
+        return remote(block, block, gp_s, gp_r.at[k], partner)
+
+    def p2_copy(k, i):
+        cols = pl.ds(i * side, side)
+        return remote(
+            contrib.at[k, 1 - core, :, :, cols],
+            pair2.at[k, :, :, cols],
+            p2_s,
+            p2_r.at[k, i],
+            partner,
+        )
 
     def r1_copy(k, i):
         owner, target, first = (
@@ -350,14 +395,19 @@
         )[i]
         cols = pl.ds(0, side) if first else pl.ds(side, side)
         return remote(
-            red.at[k, owner, :, cols], r1.at[k, i], r1_s.at[k, i], r1_r.at[k, i], target
+            red.at[k, owner, :, cols], r1.at[k, i], r1_s, r1_r.at[k, min(i, 2)], target
         )
 
     def r2_copy(k, i):
-        return remote(mid.at[k, i], r2.at[k, i], r2_s.at[k, i], r2_r.at[k, i], (to_y, to_x)[i])
+        return remote(mid.at[k, i], r2.at[k, i], r2_s, r1_r.at[k, 2], (to_y, to_x)[i])
 
     def z2_copy(k):
-        return remote(z2s.at[k], z2.at[k], z2_s.at[k], z2_r.at[k], to_z(-(k % (nz - 1) + 1)))
+        base = far_steps(k // nz)[0]
+        owner = owner_of(k - base)
+        there = base + rank(owner, z)
+        return remote(
+            z2s.at[k], z2.at[there], z2_s, z2_r.at[k // nz], {"sp": sp, "tp": owner * 2 + core}
+        )
 
     moves = (
         (kb_hbm, kb_raw),
@@ -478,8 +528,7 @@
 
     for load in loads[6:10]:
         load.wait()
-    for i in range(2, 6):
-        kv_copy(0, i).wait_recv()
+    settle(kv_all.at[0, 0:2], kv_r.at[0, 2])
     for h in range(heads):
         att_b[:, h * vb : (h + 1) * vb] = attend(
             0,
@@ -497,8 +546,7 @@
             kv_copy(p, i).wait_recv()
             kv_copy(p, 4 + i).start()
     for h in range(heads - 1):
-        for i in range(2, 6):
-            kv_copy(1 + h, i).wait_recv()
+        settle(kv_all.at[1 + h, 0:2], kv_r.at[1 + h, 2])
         attend_a(h)
     tile, group = 512, 4
     known = (heads - 1) * va
@@ -511,8 +559,7 @@
                 att_a[:, :known], out_a[:known, cols], preferred_element_type=f32
             ) + jnp.dot(att_b[...], out_b[:, cols], preferred_element_type=f32)
 
-    for i in range(2, 6):
-        kv_copy(heads, i).wait_recv()
+    settle(kv_all.at[heads, 0:2], kv_r.at[heads, 2])
     attend_a(heads - 1)
 
     @pl.loop(0, width // (tile * group))
@@ -548,27 +595,27 @@
 
     def normalise(h):
         total = tot[h]
+        settle(z1.at[h], z1_r.at[h])
         for d in range(1, nz):
-            z1_copy(h, d).wait_recv()
             total += z1[h, d - 1].astype(f32)
         here_rows = slice(h * band, (h + 1) * band)
         mix = (res[here_rows].astype(f32) + total).astype(bf16)
         mixed[h] = mix
         full = mix.astype(f32)
         scaled = lax.rsqrt(jnp.mean(full * full, axis=1, keepdims=True) + EPSILON)
-        x_all[step_of(h, 0), sp, core, :, :width] = (full * scaled * norm[...]).astype(bf16)
+        x_all[own_step(h), sp, core, :, :width] = (full * scaled * norm[...]).astype(bf16)
         weights = route[here_rows]
         high = weights.astype(bf16).astype(f32)
         at = lax.broadcasted_iota(jnp.int32, weights.shape, 1)
-        x_all[step_of(h, 0), sp, core, :, width:] = jnp.where(
+        x_all[own_step(h), sp, core, :, width:] = jnp.where(
             at < experts_all, high, weights - high
         ).astype(bf16)
-        for d in range(1, nz):
-            gz_copy(h, d).start()
+        spread_z(h, lambda copy: copy.start())
 
     def arrive(k):
         block = x_all.at[k, sp, core]
         remote(block, block, gz_s.at[k], gz_r.at[k], to_z(1)).wait_recv()
+        pass_on(k, lambda copy: copy.start())
 
     def open_step(k):
         for i in range(4):
@@ -581,18 +628,13 @@
             gs_copy(k, 4 + i).start()
 
     def collect(k):
-        gs_copy(k, 2).wait_recv()
-        gp_copy(k, 1).start()
-        gs_copy(k, 3).wait_recv()
-        gp_copy(k, 2).start()
-        gs_copy(k, 4).wait_recv()
-        gs_copy(k, 5).wait_recv()
-        gp_copy(k, 3).start()
+        settle(x_all.at[k, 0:2, 0], gs_r.at[k, 2])
+        for e in range(1, 4):
+            gp_copy(k, e).start()
 
     def compute(q):
-        for i in range(2):
-            for e in range(4):
-                gp_copy(2 * q + i, e).wait_recv()
+        for t in range(2):
+            settle(x_all.at[2 * q + t, :, 0], gp_r.at[2 * q + t])
         both = pl.ds(2 * q, 2)
         share = x_all[both, :, :, :, width:].reshape(chunk, lanes).astype(f32)
         at = lax.broadcasted_iota(jnp.int32, share.shape, 1)
@@ -611,11 +653,9 @@
                 clamped * jax.nn.sigmoid(SLOPE * clamped) * (jnp.clip(upward, -LIMIT, LIMIT) + 1.0)
             )
             act[:, j * hidden : (j + 1) * hidden] = (active * weight).astype(bf16)
-
-        @pl.loop(0, width // (tile * group))
-        def _(i):
-            for g in range(group):
-                cols = pl.ds(pl.multiple_of((i * group + g) * tile, tile), tile)
+        for i in range(2):
+            for g in range(side // tile):
+                cols = slice(i * side + g * tile, i * side + (g + 1) * tile)
                 rowsum = jnp.zeros((chunk, tile), f32)
                 for j in range(experts_here):
                     rowsum += jnp.dot(
@@ -629,9 +669,8 @@
                         for c in range(2):
                             r = ((t * n_sp + s) * 2 + c) * band
                             contrib[2 * q + t, c, s, :, cols] = value[r : r + band]
-
-        for i in range(2):
-            p2_copy(2 * q + i).start()
+            for t in range(2):
+                p2_copy(2 * q + t, i).start()
 
     first_cols, last_cols = slice(0, side), slice(side, 2 * side)
 
@@ -641,12 +680,13 @@
         ).astype(bf16)
 
     def reduce_out(k):
-        p2_copy(k).wait_recv()
+        p2_copy(k, 0).wait_recv()
         join(k, corner, first_cols)
         r1_copy(k, 0).start()
+        join(k, x_next, first_cols)
+        p2_copy(k, 1).wait_recv()
         join(k, corner, last_cols)
         r1_copy(k, 1).start()
-        join(k, x_next, first_cols)
         r1_copy(k, 2).start()
         join(k, y_next, last_cols)
         r1_copy(k, 3).start()
@@ -662,105 +702,77 @@
         r2_copy(k, 1).start()
 
     def reduce_in(k):
+        h, own = k // nz, k == own_step(k // nz)
+        settle(r1.at[k], r1_r.at[k, 2])
         for i, cols in enumerate((first_cols, last_cols)):
             total = contrib[k, core, sp, :, cols].astype(f32) + pair2[k, sp, :, cols].astype(f32)
-            r1_copy(k, 2 + i).wait_recv()
-            r2_copy(k, i).wait_recv()
             total += r1[k, 2 + i].astype(f32) + r2[k, i].astype(f32)
-
-            @pl.when(k < distant)
+            if own:
+                home[h, :, cols] = total
+            else:
+                z2s[k, :, cols] = total.astype(bf16)
+        if not own:
+            z2_copy(k).start()
+
+    def second_half():
+        for d in range(1, nz):
+            z1_copy(1, d).start()
+
+    def weights_in():
+        for load in loads[12:]:
+            load.wait()
+
+    acts = {
+        "n": normalise,
+        "a": arrive,
+        "o": open_step,
+        "f": relay,
+        "c": collect,
+        "r": reduce_out,
+        "m": reduce_mid,
+        "i": reduce_in,
+    }
+    def follow(words):
+        for word in (word for part in words for word in part.split()):
+            if word == "z":
+                second_half()
+            elif word == "w":
+                weights_in()
+            else:
+                acts[word[0]](int(word[1]))
+
+    @pl.loop(0, steps // 2)
+    def _(q):
+        for i in range(steps // 2):
+
+            @pl.when(q == i)
             def _():
-                z2s[k, :, cols] = total.astype(bf16)
-
-            @pl.when(k >= distant)
-            def _():
-                home[k - distant, :, cols] = total
-
-        @pl.when(k < distant)
-        def _():
-            z2_copy(k).start()
-
-    normalise(0)
-    open_step(distant)
-    for d in range(1, nz):
-        z1_copy(1, d).start()
-    arrive(0)
-    open_step(0)
-    relay(distant)
-    arrive(1)
-    open_step(1)
-    relay(0)
-    for load in loads[12:]:
-        load.wait()
-
-    @pl.loop(0, steps + 4)
-    def _(k):
-        @pl.when(k + 2 < distant)
-        def _():
-            arrive(k + 2)
-            open_step(k + 2)
-
-        @pl.when(k + 1 < distant)
-        def _():
-            relay(k + 1)
-
-        @pl.when(k == 2)
-        def _():
-            relay(distant + 1)
-
-        @pl.when(k < steps)
-        def _():
-            collect(k)
-
-        @pl.when((k >= 2) & (k - 2 < steps))
-        def _():
-            reduce_out(k - 2)
-
-        @pl.when((k >= 3) & (k - 3 < steps))
-        def _():
-            reduce_mid(k - 3)
-
-        @pl.when(k >= 4)
-        def _():
-            reduce_in(k - 4)
-
-        @pl.when(k == 0)
-        def _():
-            normalise(1)
-            open_step(distant + 1)
-
-        @pl.when((k < steps) & (k % 2 == 1))
-        def _():
-            compute(k // 2)
+                follow(PLAN[i])
+
+        compute(q)
+
+    follow(PLAN[-1])
 
     for h in range(halves):
         total = mixed[h].astype(f32) + home[h]
-        for d in range(1, nz):
-            k = step_of(h, d)
-            z2_copy(k).wait_recv()
+        settle(z2.at[0 : nz - 1], z2_r.at[h])
+        for k in far_steps(h):
             total += z2[k].astype(f32)
         o_ref[h * band : (h + 1) * band, :] = total.astype(bf16)
 
-    for p in range(1 + heads):
-        for i in range(6):
-            kv_copy(p, i).wait_send()
+    settle(kv_all.at[:, 0 : n_sp - 1], kv_s)
+    settle(pair1, p1_s)
+    settle(z1, z1_s)
+    settle(x_all.at[:, 0 : n_sp - 1, 0], gs_s)
+    settle(x_all.at[:, :, 0], gp_s)
+    settle(pair2, p2_s)
+    settle(r1, r1_s)
+    settle(r2, r2_s)
+    settle(z2.at[0 : halves * (nz - 1)], z2_s)
     for h in range(halves):
-        p1_copy(h).wait_send()
-        for d in range(1, nz):
-            z1_copy(h, d).wait_send()
-            gz_copy(h, d).wait_send()
-            z2_copy(step_of(h, d)).wait_send()
-
-    @pl.loop(0, steps)
-    def _(k):
-        for i in range(6):
-            gs_copy(k, i).wait_send()
-        for e in range(4):
-            gp_copy(k, e).wait_send()
-            r1_copy(k, e).wait_send()
-        p2_copy(k).wait_send()
-        for i in range(2):
-            r2_copy(k, i).wait_send()
+        spread_z(h, lambda copy: copy.wait_send())
+        for k in far_steps(h):
+            pass_on(k, lambda copy: copy.wait_send())
 
 
 def per_device(
@@ -809,8 +821,8 @@
     hbm = pl.BlockSpec(memory_space=pl.ANY)
     smem = pl.BlockSpec(memory_space=pltpu.SMEM)
     sem = pltpu.SemaphoreType.DMA
-    pairs = [(1 + heads, 6), (halves,), (halves, nz - 1), (halves * (nz - 1),), (steps, 6)]
-    pairs += [(steps, 4), (steps,), (steps, 4), (steps, 2), (halves * (nz - 1),)]
+    waits = [(), (1 + heads, 3), (), (halves,), (), (halves,), (steps + 2 * halves,), (steps,)]
+    waits += [(), (steps, 3), (), (steps,), (), (steps, 2), (), (steps, 3), (), (), (halves,)]
     scratch = [pltpu.VMEM(a.shape, bf16) for a in streams]
     scratch += [
         pltpu.VMEM((1, va), f32),
@@ -845,12 +857,11 @@
         pltpu.VMEM((steps, 2, band, width // 2), bf16),
         pltpu.VMEM((steps, 2, band, width // 2), bf16),
         pltpu.VMEM((halves, band, width), f32),
-        pltpu.VMEM((halves * (nz - 1), band, width), bf16),
-        pltpu.VMEM((halves * (nz - 1), band, width), bf16),
+        pltpu.VMEM((steps, band, width), bf16),
+        pltpu.VMEM((steps, band, width), bf16),
         sem((15,)),
     ]
-    for shape in pairs:
-        scratch += [sem(shape), sem(shape)]
+    scratch += [sem(shape) for shape in waits]
     return pl.pallas_call(
         functools.partial(layer_kernel, (n_sp, n_tp, heads, da, db, va, vb)),
         out_shape=jax.ShapeDtypeStruct((rows, width), bf16),

time: 90.9 us -> 79.4 us (0.87)
  Pallas kernels: 89.1 us -> 77.7 us
    pallas_call x1, Pallas kernels: 89.1 us -> 77.7 us  [per_device(): pl.pallas_call(functools.partial(layer_kernel, (n_sp, n_tp, heads, da, db...]
where the time goes in v2:
time: 79.4 us; the launch traced here: 79.3 us
  Pallas kernels  77.7 us (98%)
  local copies, waits for them, and re-layouts  1.57 us (2%)
    pallas_call x1, Pallas kernels, per_device(): pl.pallas_call(functools.partial(layer_kernel, (n_sp, n_tp, heads, da, db...  77.7 us

profile of v2, /device:TPU:0, one launch (start us, length us, event | category | flops | bytes accessed | tf_op | source)
XLA Modules:
  0.0 79.3 jit_solution(13211819698609438884)
XLA Ops:
  0.0 77.7 %shard_map.172 = bf16[16,4096]{1,0:T(8,128)(2,1)} custom-call(f32[2,2]{1,0:T(2,128)} %lam_ref.1, s32[2,16]{1,0:T(2,128)} %bitcast.30, f32[2,16]{1,0:T(2,128)} %bitcast.31, bf16[512,128]{1,0:T(8,128)(2,1)} %bitcast.23, bf16[512,128]{1,0:T(8,128)(2,1)} %bitcast.24, bf16[512,128]{1,0:T(8,128)(2,1)} %bitcast.25, bf16[256,128]{1,0:T(8,128)(2,1)} %bitcast.26, ...), custom_call_target="tpu_custom_call" | custom-call | tf_op jit(solution)/shard_map/pallas_call | solution.py:865
  77.7 1.6 %copy.23 = bf16[16,4096]{1,0:T(8,128)(2,1)} copy(bf16[16,4096]{1,0:T(8,128)(2,1)} %shard_map.172) | data formatting | bytes 262144

commit v3 on v2

--- a/solution.py
+++ b/solution.py
@@ -326,8 +326,11 @@
         place = kv_all.at[p, owner, pl.ds(half * size, size)]
         return remote(place, place, kv_s, kv_r.at[p, min(i, 2)], target)
 
-    def p1_copy(h):
-        return remote(part.at[h, 1 - core], pair1.at[h], p1_s, p1_r.at[h], partner)
+    def p1_copy(h, i):
+        cols = pl.ds(pl.multiple_of(i * side, side), side)
+        return remote(
+            part.at[h, 1 - core, :, :, cols], pair1.at[h, :, :, cols], p1_s, p1_r.at[h], partner
+        )
 
     def z1_copy(h, d):
         return remote(
@@ -545,29 +548,24 @@
         for i in range(2):
             kv_copy(p, i).wait_recv()
             kv_copy(p, 4 + i).start()
-    for h in range(heads - 1):
+    tile = 512
+
+    @pl.loop(0, 2)
+    def _(i):
+        for g in range(side // tile):
+            cols = pl.ds(pl.multiple_of(i * side + g * tile, tile), tile)
+            acc[:, cols] = jnp.dot(att_b[...], out_b[:, cols], preferred_element_type=f32)
+
+    for h in range(heads):
         settle(kv_all.at[1 + h, 0:2], kv_r.at[1 + h, 2])
         attend_a(h)
-    tile, group = 512, 4
-    known = (heads - 1) * va
-
-    @pl.loop(0, width // (tile * group))
+
+    @pl.loop(0, 2)
     def _(i):
-        for g in range(group):
-            cols = pl.ds(pl.multiple_of((i * group + g) * tile, tile), tile)
-            acc[:, cols] = jnp.dot(
-                att_a[:, :known], out_a[:known, cols], preferred_element_type=f32
-            ) + jnp.dot(att_b[...], out_b[:, cols], preferred_element_type=f32)
-
-    settle(kv_all.at[heads, 0:2], kv_r.at[heads, 2])
-    attend_a(heads - 1)
-
-    @pl.loop(0, width // (tile * group))
-    def _(i):
-        for g in range(group):
-            cols = pl.ds(pl.multiple_of((i * group + g) * tile, tile), tile)
+        for g in range(side // tile):
+            cols = pl.ds(pl.multiple_of(i * side + g * tile, tile), tile)
             value = acc[:, cols] + jnp.dot(
-                att_a[:, known:], out_a[known:, cols], preferred_element_type=f32
+                att_a[...], out_a[:, cols], preferred_element_type=f32
             )
             value = value.astype(bf16)
             for zz in range(nz):
@@ -575,14 +573,14 @@
                     for h in range(halves):
                         r = (zz * 2 + c) * rows + h * band
                         part[h, c, zz, :, cols] = value[r : r + band]
-
-    for h in range(halves):
-        p1_copy(h).start()
+        for h in range(halves):
+            p1_copy(h, i).start()
+
     loads[10].wait()
     loads[11].wait()
 
     def fold(h):
-        p1_copy(h).wait_recv()
+        settle(pair1.at[h], p1_r.at[h])
         for d in range(1, nz):
             zz = z_at(d)
             sum1[h, zz] = (part[h, core, zz].astype(f32) + pair1[h, zz].astype(f32)).astype(bf16)

time: 79.4 us -> 78.9 us (level)
  no operation moved by 1% of the time
where the time goes in v3:
time: 78.9 us; the launch traced here: 78.7 us
  Pallas kernels  77.1 us (98%)
  local copies, waits for them, and re-layouts  1.57 us (2%)
    pallas_call x1, Pallas kernels, per_device(): pl.pallas_call(functools.partial(layer_kernel, (n_sp, n_tp, heads, da, db...  77.1 us

profile of v3, /device:TPU:0, one launch (start us, length us, event | category | flops | bytes accessed | tf_op | source)
XLA Modules:
  0.0 78.7 jit_solution(695141158039240461)
XLA Ops:
  0.0 77.1 %shard_map.172 = bf16[16,4096]{1,0:T(8,128)(2,1)} custom-call(f32[2,2]{1,0:T(2,128)} %lam_ref.1, s32[2,16]{1,0:T(2,128)} %bitcast.30, f32[2,16]{1,0:T(2,128)} %bitcast.31, bf16[512,128]{1,0:T(8,128)(2,1)} %bitcast.23, bf16[512,128]{1,0:T(8,128)(2,1)} %bitcast.24, bf16[512,128]{1,0:T(8,128)(2,1)} %bitcast.25, bf16[256,128]{1,0:T(8,128)(2,1)} %bitcast.26, ...), custom_call_target="tpu_custom_call" | custom-call | tf_op jit(solution)/shard_map/pallas_call | solution.py:863
  77.2 1.6 %copy.23 = bf16[16,4096]{1,0:T(8,128)(2,1)} copy(bf16[16,4096]{1,0:T(8,128)(2,1)} %shard_map.172) | data formatting | bytes 262144
